TPU v7x, 512 devices: a whole 4x8x8 slice. The times are simulated.
512 devices in a mesh: ep: 32 (over z, x), tp: 16 (over y, core).
Axes of the slice: x: 4, y: 8, z: 8, core: 2. Of those that a mesh axis runs over, the one named last changes fastest.
Arguments:
- residual: bfloat16 [256, 2048], P(None, 'ep'), may hold values from -40 to 40
- norm_gain: float32 [2048], P('ep'), may hold values from 0.1 to 1.9
- query_weight: bfloat16 [2048, 2048], P('ep', 'tp'), may hold values from -0.125 to 0.125
- key_weight: bfloat16 [2048, 2048], P('ep', 'tp'), may hold values from -0.125 to 0.125
- value_weight: bfloat16 [2048, 4096], P('ep', 'tp'), may hold values from -0.125 to 0.125
- gate_weight: bfloat16 [2048, 4096], P('ep', 'tp'), may hold values from -0.125 to 0.125
- out_weight: bfloat16 [4096, 2048], P('tp', 'ep'), may hold values from -0.09375 to 0.09375
- prior_state: float32 [256, 16, 128, 256], P('ep', 'tp'), may hold values from -3 to 3
- lengths: int32 [256], P('ep'), may hold values from 1024 to 16383
- ffn_gain: float32 [2048], replicated, may hold values from 0.1 to 1.9
- expert_gate: bfloat16 [32, 2048, 2048], P('ep', None, 'tp'), may hold values from -0.5 to 0.5
- expert_up: bfloat16 [32, 2048, 2048], P('ep', None, 'tp'), may hold values from -0.5 to 0.5
- expert_down: bfloat16 [32, 2048, 2048], P('ep', 'tp'), may hold values from -0.03125 to 0.03125
- route_ids: int32 [256, 4], replicated, may hold values from 0 to 31, all different within a row; in each aligned block of 8 rows (0 to 7, 8 to 15, ...) at most 2 rows name the same one
- route_weight: float32 [256, 4], replicated, may hold values from 0.1 to 1
- dense_gate: bfloat16 [2048, 2048], P('ep', 'tp'), may hold values from -0.125 to 0.125
- dense_up: bfloat16 [2048, 2048], P('ep', 'tp'), may hold values from -0.125 to 0.125
- dense_down: bfloat16 [2048, 2048], P('tp', 'ep'), may hold values from -0.25 to 0.25
- mix_vector: bfloat16 [2048], P('ep'), may hold values from -0.125 to 0.125
Outputs:
- layer_out: bfloat16 [256, 2048], P(None, 'ep')
- new_state: float32 [256, 16, 128, 256], P('ep', 'tp')
Inputs may be any that keep to these rules, and one draw needn't show every extreme that they name: `route_ids`: each row names 4 different experts; within each aligned block of 8 rows no expert is named by more than 2 rows, and in some block one expert is named by exactly 2 rows.
All inputs are finite; a program needn't handle non-finite values.
Results may differ from a plain program's by a relative error of at most 0.02.
Values may be sent and summed in bfloat16 or wider, within the bound.
No kernel may reach another device: no remote copies, remote signals or barrier semaphores. Data moves between devices by JAX's collectives and lax.ppermute only.
A program may use at most 64 MiB of HBM per device.

v0:
```python
import math
import jax
import jax.numpy as jnp
from jax import lax
from jax.sharding import PartitionSpec as P

D = 2048
KEY_DIM = 128
VAL_DIM = 256
norm_eps = 1e-06
clamp_limit = 7.0
gate_alpha = 1.702


def split_up(value, dim, peers):
    shape = value.shape
    pieces = value.reshape(*shape[:dim], peers, shape[dim] // peers, *shape[dim + 1 :])
    return jnp.moveaxis(pieces, dim, 0)


def summed_on_arrival(value, axis, dim):
    pieces = split_up(value, dim, lax.axis_size(axis))
    arrived = lax.all_to_all(pieces, axis, split_axis=0, concat_axis=0, tiled=True)
    return arrived.sum(axis=0)


def in_one_piece(arrays, axis, dim, along):
    widths = [math.prod(a.shape[along:]) for a in arrays]
    both = jnp.concatenate(
        [a.reshape(*a.shape[:along], w) for a, w in zip(arrays, widths)], axis=along
    )
    filled = summed_on_arrival(both, axis, dim)
    pieces = jnp.split(filled, [sum(widths[:k]) for k in range(1, len(widths))], axis=along)
    return tuple(
        (b.reshape(*filled.shape[:along], *a.shape[along:]) for a, b in zip(arrays, pieces))
    )


def from_everyone(value, axis):
    peers = lax.axis_size(axis)
    return lax.all_to_all(
        jnp.broadcast_to(value[None], (peers, *value.shape)), axis, 0, 0, tiled=True
    )


def laid_out(pieces, dim):
    shape = list(pieces.shape[1:])
    shape[dim] *= pieces.shape[0]
    return jnp.moveaxis(pieces, 0, dim).reshape(shape)


def gather_directly(value, axis, dim):
    pieces = from_everyone(value, axis)
    return laid_out(pieces, dim)


def total_of_pieces(value, axis):
    pieces = lax.all_gather(value, axis).astype(jnp.float32)
    return pieces.sum(axis=0)


def sum_at_owner(value, axis, dim):
    pieces = split_up(value, dim, lax.axis_size(axis))
    arrived = lax.all_to_all(pieces, axis, split_axis=0, concat_axis=0, tiled=True)
    return arrived.astype(jnp.float32).sum(axis=0)


def padded_to(lines, peers):
    spare = -lines.shape[0] % peers
    if not spare:
        return lines
    return jnp.concatenate([lines, jnp.zeros((spare, *lines.shape[1:]), lines.dtype)])


def nested_sum(value, axes):
    lines = value.reshape(-1, value.shape[-1])
    own = sum_at_owner(padded_to(lines, lax.axis_size(axes)), axes, 0)
    whole = gather_directly(own.astype(jnp.bfloat16), axes, 0)
    return whole[: len(lines)].reshape(value.shape).astype(jnp.float32)


def sum_by_parts(value, axes):
    padded = padded_to(value, lax.axis_size(axes))
    whole = gather_directly(summed_on_arrival(padded, axes, 0), axes, 0)
    return lax.slice_in_dim(whole, 0, len(value)).reshape(value.shape)


def in_one(arrays, axis):
    ends = [0]
    for a in arrays:
        ends.append(ends[-1] + a.size)
    subtotal = sum_by_parts(jnp.concatenate([a.ravel() for a in arrays]), axis)
    return tuple((subtotal[b:e].reshape(a.shape) for a, b, e in zip(arrays, ends, ends[1:])))


def rotate_half(vectors, positions):
    half_dim = vectors.shape[-1] // 2
    inverse = 1.0 / 10000.0 ** jnp.linspace(0.0, 1.0, half_dim, dtype=jnp.float32)
    angles = positions.astype(jnp.float32)[:, None] * inverse[None, :]
    cosine = jnp.cos(angles)[:, None, :]
    sine_part = jnp.sin(angles)[:, None, :]
    first_half = vectors[..., :half_dim]
    second_half = vectors[..., half_dim:]
    return jnp.concatenate(
        [
            first_half * cosine - second_half * sine_part,
            second_half * cosine + first_half * sine_part,
        ],
        axis=-1,
    )


def slot_index(route_ids, groups, capacity, experts):
    pair_ids = route_ids.reshape(groups, -1)
    labels = jnp.arange(experts, dtype=jnp.int32)
    onehot = (pair_ids[:, :, None] == labels[None, None, :]).astype(jnp.int32)
    earlier = jnp.cumsum(onehot, axis=1) - onehot
    within = jnp.sum(earlier * onehot, axis=2)
    offset = jnp.arange(groups, dtype=jnp.int32)[:, None] * capacity
    return (pair_ids * (groups * capacity) + offset + within).reshape(-1)


def source_rows(target, total_rows, topk_count, table_size):
    owners = jnp.arange(target.shape[0], dtype=jnp.int32) // topk_count
    return jnp.full((table_size,), total_rows, jnp.int32).at[target].set(owners)


def rounded_product(left_rows, right_rows):
    partial_value = jnp.dot(left_rows, right_rows, preferred_element_type=jnp.float32)
    return lax.optimization_barrier(partial_value.astype(jnp.bfloat16))


def per_device(
    residual,
    norm_gain,
    query_weight,
    key_weight,
    value_weight,
    gate_weight,
    out_weight,
    prior_state,
    lengths,
    ffn_gain,
    expert_gate,
    expert_up,
    expert_down,
    route_ids,
    route_weight,
    dense_gate,
    dense_up,
    dense_down,
    mix_vector,
):
    ep_count = lax.axis_size("ep")
    ep_index = lax.axis_index("ep")
    batch_rows, local_width = residual.shape
    own_rows = batch_rows // ep_count
    topk_count = route_ids.shape[1]
    residual_float = residual.astype(jnp.float32)
    squares = jnp.sum(residual_float * residual_float, axis=1)
    normed_in = (residual_float * norm_gain).astype(jnp.bfloat16)
    all_weights = jnp.concatenate([query_weight, key_weight, value_weight, gate_weight], axis=1)
    whole_terms = jnp.dot(normed_in, all_weights, preferred_element_type=jnp.float32)
    projected, own_squares = in_one_piece((whole_terms, squares), "ep", 0, 1)
    row_scale = lax.rsqrt(own_squares / D + norm_eps)[:, None]
    key_cols = query_weight.shape[1]
    value_cols = value_weight.shape[1]
    heads_here = key_cols // KEY_DIM
    projected = projected * row_scale
    query_rot = rotate_half(projected[:, :key_cols].reshape(own_rows, heads_here, KEY_DIM), lengths)
    key_rot = rotate_half(
        projected[:, key_cols : 2 * key_cols].reshape(own_rows, heads_here, KEY_DIM), lengths
    ) * KEY_DIM ** (-0.5)
    values = projected[:, 2 * key_cols : 2 * key_cols + value_cols].reshape(
        own_rows, heads_here, VAL_DIM
    )
    gate_pre = projected[:, 2 * key_cols + value_cols :].reshape(own_rows, heads_here, VAL_DIM)
    head_ids = lax.axis_index("tp") * heads_here + jnp.arange(heads_here, dtype=jnp.int32)
    decay_rate = 1.0 - jnp.exp2(-1.0 - 0.5 * head_ids.astype(jnp.float32))
    new_state = (
        decay_rate[None, :, None, None] * prior_state
        + key_rot[:, :, :, None] * values[:, :, None, :]
    )
    state_read = jnp.einsum("bhk,bhkv->bhv", query_rot, new_state, precision=lax.Precision.HIGHEST)
    normed = state_read * lax.rsqrt(
        jnp.mean(state_read * state_read, axis=-1, keepdims=True) + norm_eps
    )
    gated_out = (
        (normed * jax.nn.silu(gate_pre))
        .astype(jnp.bfloat16)
        .reshape(own_rows, heads_here * VAL_DIM)
    )
    head_terms = rounded_product(gather_directly(gated_out, "ep", 0), out_weight)
    attn_out = total_of_pieces(head_terms.astype(jnp.float32).astype(jnp.bfloat16), "tp").astype(
        jnp.float32
    )
    after_mixer = (residual_float + attn_out).astype(jnp.bfloat16)
    capacity = max(2, 2 * own_rows * topk_count // ep_count)
    slot_count = ep_count * capacity
    target = slot_index(route_ids, ep_count, capacity, ep_count)
    slot_source = source_rows(target, batch_rows, topk_count, ep_count * slot_count)
    padded = jnp.concatenate([after_mixer, jnp.zeros((1, local_width), jnp.bfloat16)], axis=0)
    outgoing = padded[slot_source].reshape(ep_count, slot_count, local_width)
    arrived = lax.all_to_all(outgoing, "ep", split_axis=0, concat_axis=2, tiled=True)[0]
    rows_float = arrived.astype(jnp.float32)
    row_norm = lax.rsqrt(jnp.mean(rows_float * rows_float, axis=1, keepdims=True) + norm_eps)
    normed_rows = (rows_float * ffn_gain).astype(jnp.bfloat16)
    gate_val = jnp.minimum(
        jnp.dot(normed_rows, expert_gate[0], preferred_element_type=jnp.float32) * row_norm,
        clamp_limit,
    )
    up_val = jnp.clip(
        jnp.dot(normed_rows, expert_up[0], preferred_element_type=jnp.float32) * row_norm,
        -clamp_limit,
        clamp_limit,
    )
    hidden = ((up_val + 1.0) * gate_val * jax.nn.sigmoid(gate_alpha * gate_val)).astype(
        jnp.bfloat16
    )
    expert_part = rounded_product(hidden, expert_down[0]).astype(jnp.float32)
    expert_sum = nested_sum(expert_part.astype(jnp.bfloat16), "tp").astype(jnp.bfloat16)
    returned = lax.all_to_all(expert_sum[None], "ep", split_axis=2, concat_axis=0, tiled=True)
    picked = returned.reshape(ep_count * slot_count, local_width)[target]
    picked = picked.reshape(batch_rows, topk_count, local_width).astype(jnp.float32)
    routed = jnp.sum(picked * route_weight[:, :, None], axis=1)
    after_float = after_mixer.astype(jnp.float32)
    gain_here = lax.dynamic_slice_in_dim(ffn_gain, ep_index * local_width, local_width, 0)
    normed_ffn = (after_float * gain_here).astype(jnp.bfloat16)
    dense_cols = dense_gate.shape[1]
    both_terms = jnp.dot(
        normed_ffn,
        jnp.concatenate([dense_gate, dense_up], axis=1),
        preferred_element_type=jnp.float32,
    )
    mix_term = jnp.dot(normed_ffn, mix_vector, preferred_element_type=jnp.float32)
    both_terms, ffn_squares, mix_logit = in_one(
        (both_terms, jnp.sum(after_float * after_float, axis=1), mix_term), "ep"
    )
    ffn_scale = lax.rsqrt(ffn_squares / D + norm_eps)[:, None]
    dense_act = (
        jax.nn.silu(both_terms[:, :dense_cols] * ffn_scale)
        * (both_terms[:, dense_cols:] * ffn_scale)
    ).astype(jnp.bfloat16)
    dense_part = rounded_product(dense_act, dense_down).astype(jnp.float32)
    dense_out = total_of_pieces(dense_part.astype(jnp.bfloat16), "tp").astype(jnp.float32)
    dense_mix = jax.nn.sigmoid(ffn_scale[:, 0] * mix_logit)
    layer_out = (after_float + routed + dense_mix[:, None] * dense_out).astype(jnp.bfloat16)
    return (layer_out, new_state)


def solution(mesh):
    placed = (
        P(None, "ep"),
        P("ep"),
        P("ep", "tp"),
        P("ep", "tp"),
        P("ep", "tp"),
        P("ep", "tp"),
        P("tp", "ep"),
        P("ep", "tp", None, None),
        P("ep"),
        P(),
        P("ep", None, "tp"),
        P("ep", None, "tp"),
        P("ep", "tp", None),
        P(),
        P(),
        P("ep", "tp"),
        P("ep", "tp"),
        P("tp", "ep"),
        P("ep"),
    )
    return jax.shard_map(
        per_device,
        mesh=mesh,
        in_specs=placed,
        out_specs=(P(None, "ep"), P("ep", "tp", None, None)),
        check_vma=False,
    )
```

profile of v0, /device:TPU:1, one launch (start us, length us, event | category | flops | bytes accessed | tf_op | source)
XLA Modules:
  0.0 217.2 jit_solution(9277276090891454630)
XLA Ops:
  0.6 0.9 copy.80
  2.0 0.5 copy-done.5
  2.7 1.0 pad_maximum_fusion
  3.7 13.8 %all-to-all-start = ((f32[32,8,769]{2,1,0:T(8,128)}), f32[32,8,769]{2,1,0:T(8,128)S(1)}, u32[]{:S(2)}, u32[]{:S(2)}) async-start(f32[32,8,769]{2,1,0:T(8,128)} %pad_maximum_fusion), calls=%async_computation | async-start | bytes 1835008 | tf_op jit(solution)/shard_map/all_to_all | solution.py:23
  18.0 1.0 fusion.97
  19.7 21.4 %all-to-all-done = f32[32,8,769]{2,1,0:T(8,128)S(1)} async-done(((f32[32,8,769]{2,1,0:T(8,128)}), f32[32,8,769]{2,1,0:T(8,128)S(1)}, u32[]{:S(2)}, u32[]{:S(2)}) %all-to-all-start) | async-done | bytes 787488 | tf_op jit(solution)/shard_map/all_to_all | solution.py:23
  41.9 0.6 fusion.8
  42.7 0.7 broadcast_in_dim.13
  43.4 6.0 %all-to-all-start.1 = ((bf16[32,8,256]{2,1,0:T(8,128)(2,1)}), bf16[32,8,256]{2,1,0:T(8,128)(2,1)S(1)}, u32[]{:S(2)}, u32[]{:S(2)}) async-start(bf16[32,8,256]{2,1,0:T(8,128)(2,1)} %broadcast_in_dim.13), calls=%async_computation.1 | async-start | bytes 262144 | tf_op jit(solution)/shard_map/all_to_all | solution.py:41
  49.4 0.7 copy-done.13
  50.3 4.3 %scatter_custom_fusion = s32[2048]{0:T(1024)S(1)} fusion(s32[1024]{0:T(1024)S(1)} %bitcast.88, s32[1024]{0:T(1024)S(1)} %add_select_fusion, s32[]{:T(128)} %constant.47.clone.1), kind=kCustom, calls=%fused_computation.117 | custom fusion | bytes 8196 | tf_op jit(solution)/shard_map/scatter | solution.py:125
  54.6 4.3 %all-to-all-done.1 = bf16[32,8,256]{2,1,0:T(8,128)(2,1)S(1)} async-done(((bf16[32,8,256]{2,1,0:T(8,128)(2,1)}), bf16[32,8,256]{2,1,0:T(8,128)(2,1)S(1)}, u32[]{:S(2)}, u32[]{:S(2)}) %all-to-all-start.1) | async-done | bytes 131104 | tf_op jit(solution)/shard_map/all_to_all | solution.py:41
  59.0 22.2 %all-gather = bf16[4096,64]{0,1:T(8,128)(2,1)S(1)} all-gather(bf16[256,64]{0,1:T(8,128)(2,1)S(1)} %convolution_convert_fusion.2), channel_id=2, replica_groups=mesh['ep'=32,'tp'=16] {'tp'}, dimensions={0}, use_global_device_ids=true | all-gather | bytes 557056 | tf_op jit(solution)/shard_map/all_gather | solution.py:58
  82.1 0.6 copy-done.10
  83.0 0.5 copy-done.18
  83.7 6.2 %gather_fusion = bf16[2048,64]{1,0:T(8,128)(2,1)S(1)} fusion(bf16[257,64]{1,0:T(8,128)(2,1)S(1)} %concatenate.47, s32[2048]{0:T(1024)S(1)} %fusion.55), kind=kCustom, calls=%fused_computation | custom fusion | bytes 532480 | tf_op jit(solution)/shard_map/gather | solution.py:203
  89.8 1.1 reshape.350
  90.9 4.1 %all-to-all-start.2 = ((bf16[32,2,2048]{2,1,0:T(2,128)(2,1)}), bf16[32,2,2048]{2,1,0:T(2,128)(2,1)S(1)}, u32[]{:S(2)}, u32[]{:S(2)}) async-start(bf16[32,2,2048]{2,1,0:T(2,128)(2,1)} %reshape.350), calls=%async_computation.2 | async-start | bytes 524288 | tf_op jit(solution)/shard_map/all_to_all | solution.py:204
  95.0 1.1 all_to_all.48
  96.1 10.5 %all-to-all-done.2 = bf16[32,2,2048]{2,1,0:T(2,128)(2,1)S(1)} async-done(((bf16[32,2,2048]{2,1,0:T(2,128)(2,1)}), bf16[32,2,2048]{2,1,0:T(2,128)(2,1)S(1)}, u32[]{:S(2)}, u32[]{:S(2)}) %all-to-all-start.2) | async-done | bytes 262176 | tf_op jit(solution)/shard_map/all_to_all | solution.py:204
  106.6 4.5 %all-to-all-start.6 = ((f32[32,1,2064]{2,1,0:T(1,128)}), f32[32,1,2064]{2,1,0:T(1,128)S(1)}, u32[]{:S(2)}, u32[]{:S(2)}) async-start(f32[32,1,2064]{2,1,0:T(1,128)} %all_to_all.48), calls=%async_computation.6 | async-start | bytes 557056 | tf_op jit(solution)/shard_map/all_to_all | solution.py:23
  112.2 0.4 convert_element_type.104
  112.7 0.6 copy-done.3
  113.5 0.8 copy-done.4
  114.3 0.4 convolution_convert_fusion
  114.7 0.8 reshape.301
  115.5 6.4 %all-to-all-done.6 = f32[32,1,2064]{2,1,0:T(1,128)S(1)} async-done(((f32[32,1,2064]{2,1,0:T(1,128)}), f32[32,1,2064]{2,1,0:T(1,128)S(1)}, u32[]{:S(2)}, u32[]{:S(2)}) %all-to-all-start.6) | async-done | bytes 264224 | tf_op jit(solution)/shard_map/all_to_all | solution.py:23
  121.9 7.8 %all-to-all-start.3 = ((bf16[16,4,2048]{2,1,0:T(4,128)(2,1)}), bf16[16,4,2048]{2,1,0:T(4,128)(2,1)S(1)}, u32[]{:S(2)}, u32[]{:S(2)}) async-start(bf16[16,4,2048]{2,1,0:T(4,128)(2,1)} %reshape.301), calls=%async_computation.3 | async-start | bytes 524288 | tf_op jit(solution)/shard_map/all_to_all | solution.py:64
  129.9 11.4 %all-to-all-done.3 = bf16[16,4,2048]{2,1,0:T(4,128)(2,1)S(1)} async-done(((bf16[16,4,2048]{2,1,0:T(4,128)(2,1)}), bf16[16,4,2048]{2,1,0:T(4,128)(2,1)S(1)}, u32[]{:S(2)}, u32[]{:S(2)}) %all-to-all-start.3) | async-done | bytes 262176 | tf_op jit(solution)/shard_map/all_to_all | solution.py:64
  141.3 0.8 broadcast_in_dim.18
  142.1 3.9 %all-to-all-start.7 = ((f32[32,1,2064]{2,1,0:T(1,128)}), f32[32,1,2064]{2,1,0:T(1,128)S(1)}, u32[]{:S(2)}, u32[]{:S(2)}) async-start(f32[32,1,2064]{2,1,0:T(1,128)} %broadcast_in_dim.18), calls=%async_computation.7 | async-start | bytes 557056 | tf_op jit(solution)/shard_map/all_to_all | solution.py:41
  146.1 13.0 %all-to-all-done.7 = f32[32,1,2064]{2,1,0:T(1,128)S(1)} async-done(((f32[32,1,2064]{2,1,0:T(1,128)}), f32[32,1,2064]{2,1,0:T(1,128)S(1)}, u32[]{:S(2)}, u32[]{:S(2)}) %all-to-all-start.7) | async-done | bytes 264224 | tf_op jit(solution)/shard_map/all_to_all | solution.py:41
  159.1 0.8 broadcast_in_dim.16
  159.9 3.9 %all-to-all-start.4 = ((bf16[16,4,2048]{2,1,0:T(4,128)(2,1)}), bf16[16,4,2048]{2,1,0:T(4,128)(2,1)S(1)}, u32[]{:S(2)}, u32[]{:S(2)}) async-start(bf16[16,4,2048]{2,1,0:T(4,128)(2,1)} %broadcast_in_dim.16), calls=%async_computation.4 | async-start | bytes 524288 | tf_op jit(solution)/shard_map/all_to_all | solution.py:41
  164.0 0.7 reduce.7
  165.1 10.5 %all-to-all-done.4 = bf16[16,4,2048]{2,1,0:T(4,128)(2,1)S(1)} async-done(((bf16[16,4,2048]{2,1,0:T(4,128)(2,1)}), bf16[16,4,2048]{2,1,0:T(4,128)(2,1)S(1)}, u32[]{:S(2)}, u32[]{:S(2)}) %all-to-all-start.4) | async-done | bytes 262176 | tf_op jit(solution)/shard_map/all_to_all | solution.py:41
  175.7 0.7 copy.88
  176.4 0.5 broadcast.245
  176.9 11.5 %reduce.10 = bf16[2048,64]{1,0:T(8,128)(2,1)S(1)} reduce(bf16[2048,1,64]{2,1,0:T(2,128)(2,1)S(1)} %bitcast.80, bf16[]{:T(256)} %broadcast.245), dimensions={1}, to_apply=%bitcast.71.reduce_sub_computation | reduce | bytes 524290
  188.5 1.1 reshape.352
  189.6 4.4 %all-to-all-start.5 = ((bf16[32,2,2048]{2,1,0:T(2,128)(2,1)}), bf16[32,2,2048]{2,1,0:T(2,128)(2,1)S(1)}, u32[]{:S(2)}, u32[]{:S(2)}) async-start(bf16[32,2,2048]{2,1,0:T(2,128)(2,1)} %reshape.352), calls=%async_computation.5 | async-start | bytes 524288 | tf_op jit(solution)/shard_map/all_to_all | solution.py:222
  194.2 15.9 %all-gather.1 = bf16[4096,64]{0,1:T(8,128)(2,1)S(1)} all-gather(bf16[256,64]{0,1:T(8,128)(2,1)S(1)} %convolution_convert_fusion.1), channel_id=3, replica_groups=mesh['ep'=32,'tp'=16] {'tp'}, dimensions={0}, use_global_device_ids=true | all-gather | bytes 557056 | tf_op jit(solution)/shard_map/all_gather | solution.py:58
  210.8 0.6 reshape.353
  211.4 0.6 copy.89
  212.0 0.5 all_to_all.46
  212.8 3.2 %gather_fusion.1 = bf16[1024,64]{1,0:T(8,128)(2,1)S(1)} fusion(bf16[2048,64]{1,0:T(8,128)(2,1)S(1)} %bitcast.78, s32[1024]{0:T(1024)S(1)} %broadcast_clamp_fusion), kind=kCustom, calls=%fused_computation.1 | custom fusion | bytes 266240 | tf_op jit(solution)/shard_map/gather | solution.py:223
  216.0 0.4 fusion.12
  216.5 0.7 copy.94
  (98 shorter events, 7.5 us)
Async XLA Ops:
  0.6 112.9 %copy-start = (bf16[1,128,2048]{2,1,0:T(8,128)(2,1)S(1)}, bf16[1,128,2048]{2,1,0:T(8,128)(2,1)}, u32[]{:S(2)}) copy-start(bf16[1,128,2048]{2,1,0:T(8,128)(2,1)} %param.33) | copy-start | bytes 1572868
  1.7 0.8 copy-start.5
  1.7 0.8 copy-start.6
  1.7 0.8 copy-start.8
  1.7 0.7 copy-start.9
  1.7 0.7 copy-start.15
  3.7 13.9 %copy-start.17 = (s32[8]{0:T(128)S(1)}, s32[8]{0:T(128)}, u32[]{:S(2)}) copy-start(s32[8]{0:T(128)} %param.29) | copy-start | bytes 100
  3.7 13.9 %copy-start.12 = (s32[256,4]{0,1:T(4,128)S(1)}, s32[256,4]{0,1:T(4,128)}, u32[]{:S(2)}) copy-start(s32[256,4]{0,1:T(4,128)} %param.34) | copy-start | bytes 12292
  3.7 37.4 %all-to-all-start = ((f32[32,8,769]{2,1,0:T(8,128)}), f32[32,8,769]{2,1,0:T(8,128)S(1)}, u32[]{:S(2)}, u32[]{:S(2)}) async-start(f32[32,8,769]{2,1,0:T(8,128)} %pad_maximum_fusion), calls=%async_computation | async-start | bytes 1835008 | tf_op jit(solution)/shard_map/all_to_all | solution.py:23
  17.6 24.1 %copy-start.2 = (f32[8,1,128,256]{3,2,1,0:T(8,128)S(1)}, f32[8,1,128,256]{3,2,1,0:T(8,128)}, u32[]{:S(2)}) copy-start(f32[8,1,128,256]{3,2,1,0:T(8,128)} %param.28) | copy-start | bytes 3145732
  41.9 39.3 %copy-start.1 = (f32[8,1,128,256]{3,2,1,0:T(8,128)}, f32[8,1,128,256]{3,2,1,0:T(8,128)S(1)}, u32[]{:S(2)}) copy-start(f32[8,1,128,256]{3,2,1,0:T(8,128)S(1)} %multiply_add_fusion) | copy-start | bytes 3145732
  43.4 15.4 %all-to-all-start.1 = ((bf16[32,8,256]{2,1,0:T(8,128)(2,1)}), bf16[32,8,256]{2,1,0:T(8,128)(2,1)S(1)}, u32[]{:S(2)}, u32[]{:S(2)}) async-start(bf16[32,8,256]{2,1,0:T(8,128)(2,1)} %broadcast_in_dim.13), calls=%async_computation.1 | async-start | bytes 262144 | tf_op jit(solution)/shard_map/all_to_all | solution.py:41
  49.4 0.7 copy-start.13
  49.4 9.4 %copy-start.7 = (bf16[256,64]{0,1:T(8,128)(2,1)S(1)}, bf16[256,64]{0,1:T(8,128)(2,1)}, u32[]{:S(2)}) copy-start(bf16[256,64]{0,1:T(8,128)(2,1)} %param.27) | copy-start | bytes 98308
  81.9 0.7 copy-start.10
  81.9 0.7 copy-start.11
  82.8 0.7 copy-start.18
  90.9 15.7 %all-to-all-start.2 = ((bf16[32,2,2048]{2,1,0:T(2,128)(2,1)}), bf16[32,2,2048]{2,1,0:T(2,128)(2,1)S(1)}, u32[]{:S(2)}, u32[]{:S(2)}) async-start(bf16[32,2,2048]{2,1,0:T(2,128)(2,1)} %reshape.350), calls=%async_computation.2 | async-start | bytes 524288 | tf_op jit(solution)/shard_map/all_to_all | solution.py:204
  106.6 15.3 %all-to-all-start.6 = ((f32[32,1,2064]{2,1,0:T(1,128)}), f32[32,1,2064]{2,1,0:T(1,128)S(1)}, u32[]{:S(2)}, u32[]{:S(2)}) async-start(f32[32,1,2064]{2,1,0:T(1,128)} %all_to_all.48), calls=%async_computation.6 | async-start | bytes 557056 | tf_op jit(solution)/shard_map/all_to_all | solution.py:23
  112.2 1.0 copy-start.3
  113.3 1.0 copy-start.4
  121.9 19.4 %all-to-all-start.3 = ((bf16[16,4,2048]{2,1,0:T(4,128)(2,1)}), bf16[16,4,2048]{2,1,0:T(4,128)(2,1)S(1)}, u32[]{:S(2)}, u32[]{:S(2)}) async-start(bf16[16,4,2048]{2,1,0:T(4,128)(2,1)} %reshape.301), calls=%async_computation.3 | async-start | bytes 524288 | tf_op jit(solution)/shard_map/all_to_all | solution.py:64
  142.1 17.0 %all-to-all-start.7 = ((f32[32,1,2064]{2,1,0:T(1,128)}), f32[32,1,2064]{2,1,0:T(1,128)S(1)}, u32[]{:S(2)}, u32[]{:S(2)}) async-start(f32[32,1,2064]{2,1,0:T(1,128)} %broadcast_in_dim.18), calls=%async_computation.7 | async-start | bytes 557056 | tf_op jit(solution)/shard_map/all_to_all | solution.py:41
  159.9 3.9 %copy-start.14 = (f32[256,4]{0,1:T(4,128)S(1)}, f32[256,4]{0,1:T(4,128)}, u32[]{:S(2)}) copy-start(f32[256,4]{0,1:T(4,128)} %param.35) | copy-start | bytes 12292
  159.9 15.7 %all-to-all-start.4 = ((bf16[16,4,2048]{2,1,0:T(4,128)(2,1)}), bf16[16,4,2048]{2,1,0:T(4,128)(2,1)S(1)}, u32[]{:S(2)}, u32[]{:S(2)}) async-start(bf16[16,4,2048]{2,1,0:T(4,128)(2,1)} %broadcast_in_dim.16), calls=%async_computation.4 | async-start | bytes 524288 | tf_op jit(solution)/shard_map/all_to_all | solution.py:41
  189.6 4.4 %copy-start.16 = (bf16[128,64]{0,1:T(8,128)(2,1)S(1)}, bf16[128,64]{0,1:T(8,128)(2,1)}, u32[]{:S(2)}) copy-start(bf16[128,64]{0,1:T(8,128)(2,1)} %param.38) | copy-start | bytes 49156
  189.6 21.2 %all-to-all-start.5 = ((bf16[32,2,2048]{2,1,0:T(2,128)(2,1)}), bf16[32,2,2048]{2,1,0:T(2,128)(2,1)S(1)}, u32[]{:S(2)}, u32[]{:S(2)}) async-start(bf16[32,2,2048]{2,1,0:T(2,128)(2,1)} %reshape.352), calls=%async_computation.5 | async-start | bytes 524288 | tf_op jit(solution)/shard_map/all_to_all | solution.py:222
where the time goes:
time: 218 us; the launch traced here: 217 us
  waiting for transfers between devices  77.5 us (36%)
  starting transfers between devices  48.3 us (22%)
  blocking collectives  38.1 us (17%)
  local copies, waits for them, and re-layouts  32.7 us (15%)
  other arithmetic  17.1 us (8%)
    all_gather x2, blocking collectives, total_of_pieces(): pieces = lax.all_gather(value, axis).astype(jnp.float32)  38.1 us
    all_to_all x2, waiting for transfers between devices, summed_on_arrival(): lax.all_to_all(pieces, axis, split_axis=0, concat_axis=0, tiled=True)  27.8 us
    all_to_all x3, waiting for transfers between devices, from_everyone(): lax.all_to_all(jnp.broadcast_to(value[None], (peers, *value.shape)), axis...  27.7 us
    all_to_all x2, starting transfers between devices, summed_on_arrival(): lax.all_to_all(pieces, axis, split_axis=0, concat_axis=0, tiled=True)  18.4 us
    all_to_all x3, starting transfers between devices, from_everyone(): lax.all_to_all(jnp.broadcast_to(value[None], (peers, *value.shape)), axis...  13.7 us
    unnamed x1, other arithmetic  11.5 us
    all_to_all x1, waiting for transfers between devices, sum_at_owner(): lax.all_to_all(pieces, axis, split_axis=0, concat_axis=0, tiled=True)  11.4 us
    all_to_all x1, waiting for transfers between devices, per_device(): lax.all_to_all(outgoing, 'ep', split_axis=0, concat_axis=2, tiled=True)[0]  10.5 us
  transfers between devices with their start and end apart: 8, of which 7 were waited for; matrix products, arithmetic and copies ran while one was open for 5% of the time, Pallas kernels for 0%

commit v1 on v0

--- a/solution.py
+++ b/solution.py
@@ -219,7 +219,12 @@
     )
     expert_part = rounded_product(hidden, expert_down[0]).astype(jnp.float32)
     expert_sum = nested_sum(expert_part.astype(jnp.bfloat16), "tp").astype(jnp.bfloat16)
-    returned = lax.all_to_all(expert_sum[None], "ep", split_axis=2, concat_axis=0, tiled=True)
+    returned = jnp.concatenate(
+        lax.all_to_all(
+            jnp.stack(jnp.split(expert_sum[None], lax.axis_size("ep"), axis=2)), "ep", 0, 0
+        ),
+        axis=0,
+    )
     picked = returned.reshape(ep_count * slot_count, local_width)[target]
     picked = picked.reshape(batch_rows, topk_count, local_width).astype(jnp.float32)
     routed = jnp.sum(picked * route_weight[:, :, None], axis=1)

time: 218 us -> 206 us (0.945)
  other arithmetic: 17.1 us -> 5.6 us
    unnamed x1 -> x0, other arithmetic: 11.5 us -> none
    unnamed x50 -> x80, local copies, waits for them, and re-layouts: 10.1 us -> 10.8 us
  transfers between devices with their start and end apart: 8 -> 8, of which waited for: 7 -> 7; matrix products, arithmetic and copies ran while one was open for 5% -> 6% of each run, Pallas kernels for 0% -> 0%
where the time goes in v1:
time: 206 us; the launch traced here: 204 us
  waiting for transfers between devices  77.5 us (38%)
  starting transfers between devices  48.3 us (23%)
  blocking collectives  38.1 us (18%)
  local copies, waits for them, and re-layouts  31.4 us (15%)
  other arithmetic  5.6 us (3%)
  matrix products  2.16 us (1%)
    all_gather x2, blocking collectives, total_of_pieces(): pieces = lax.all_gather(value, axis).astype(jnp.float32)  38.1 us
    all_to_all x2, waiting for transfers between devices, summed_on_arrival(): lax.all_to_all(pieces, axis, split_axis=0, concat_axis=0, tiled=True)  27.8 us
    all_to_all x3, waiting for transfers between devices, from_everyone(): lax.all_to_all(jnp.broadcast_to(value[None], (peers, *value.shape)), axis...  27.7 us
    all_to_all x2, starting transfers between devices, summed_on_arrival(): lax.all_to_all(pieces, axis, split_axis=0, concat_axis=0, tiled=True)  18.4 us
    all_to_all x3, starting transfers between devices, from_everyone(): lax.all_to_all(jnp.broadcast_to(value[None], (peers, *value.shape)), axis...  13.7 us
    all_to_all x1, waiting for transfers between devices, sum_at_owner(): lax.all_to_all(pieces, axis, split_axis=0, concat_axis=0, tiled=True)  11.4 us
    unnamed x80, local copies, waits for them, and re-layouts  10.8 us
    all_to_all x1, waiting for transfers between devices, per_device(): lax.all_to_all(outgoing, 'ep', split_axis=0, concat_axis=2, tiled=True)[0]  10.5 us
  transfers between devices with their start and end apart: 8, of which 7 were waited for; matrix products, arithmetic and copies ran while one was open for 6% of the time, Pallas kernels for 0%

profile of v1, /device:TPU:1, one launch (start us, length us, event | category | flops | bytes accessed | tf_op | source)
XLA Modules:
  0.0 204.5 jit_solution(17358102217650725900)
XLA Ops:
  0.6 0.9 copy.133
  2.0 0.5 copy-done.5
  2.7 1.0 pad_maximum_fusion
  3.7 13.8 %all-to-all-start = ((f32[32,8,769]{2,1,0:T(8,128)}), f32[32,8,769]{2,1,0:T(8,128)S(1)}, u32[]{:S(2)}, u32[]{:S(2)}) async-start(f32[32,8,769]{2,1,0:T(8,128)} %pad_maximum_fusion), calls=%async_computation | async-start | bytes 1835008 | tf_op jit(solution)/shard_map/all_to_all | solution.py:23
  18.0 1.0 fusion.97
  19.7 21.4 %all-to-all-done = f32[32,8,769]{2,1,0:T(8,128)S(1)} async-done(((f32[32,8,769]{2,1,0:T(8,128)}), f32[32,8,769]{2,1,0:T(8,128)S(1)}, u32[]{:S(2)}, u32[]{:S(2)}) %all-to-all-start) | async-done | bytes 787488 | tf_op jit(solution)/shard_map/all_to_all | solution.py:23
  41.9 0.6 fusion.8
  42.7 0.7 broadcast_in_dim.13
  43.4 6.0 %all-to-all-start.1 = ((bf16[32,8,256]{2,1,0:T(8,128)(2,1)}), bf16[32,8,256]{2,1,0:T(8,128)(2,1)S(1)}, u32[]{:S(2)}, u32[]{:S(2)}) async-start(bf16[32,8,256]{2,1,0:T(8,128)(2,1)} %broadcast_in_dim.13), calls=%async_computation.1 | async-start | bytes 262144 | tf_op jit(solution)/shard_map/all_to_all | solution.py:41
  49.4 0.7 copy-done.13
  50.3 4.3 %scatter_custom_fusion = s32[2048]{0:T(1024)S(1)} fusion(s32[1024]{0:T(1024)S(1)} %bitcast.210, s32[1024]{0:T(1024)S(1)} %add_select_fusion, s32[]{:T(128)} %constant.47.clone.1), kind=kCustom, calls=%fused_computation.181 | custom fusion | bytes 8196 | tf_op jit(solution)/shard_map/scatter | solution.py:125
  54.6 4.3 %all-to-all-done.1 = bf16[32,8,256]{2,1,0:T(8,128)(2,1)S(1)} async-done(((bf16[32,8,256]{2,1,0:T(8,128)(2,1)}), bf16[32,8,256]{2,1,0:T(8,128)(2,1)S(1)}, u32[]{:S(2)}, u32[]{:S(2)}) %all-to-all-start.1) | async-done | bytes 131104 | tf_op jit(solution)/shard_map/all_to_all | solution.py:41
  59.0 22.2 %all-gather = bf16[4096,64]{0,1:T(8,128)(2,1)S(1)} all-gather(bf16[256,64]{0,1:T(8,128)(2,1)S(1)} %convolution_convert_fusion.2), channel_id=2, replica_groups=mesh['ep'=32,'tp'=16] {'tp'}, dimensions={0}, use_global_device_ids=true | all-gather | bytes 557056 | tf_op jit(solution)/shard_map/all_gather | solution.py:58
  81.3 0.3 copy.148
  82.1 0.6 copy-done.10
  83.0 0.5 copy-done.18
  83.7 6.2 %gather_fusion = bf16[2048,64]{1,0:T(8,128)(2,1)S(1)} fusion(bf16[257,64]{1,0:T(8,128)(2,1)S(1)} %concatenate.47, s32[2048]{0:T(1024)S(1)} %fusion.55), kind=kCustom, calls=%fused_computation | custom fusion | bytes 532480 | tf_op jit(solution)/shard_map/gather | solution.py:203
  89.8 1.1 reshape.345
  90.9 4.1 %all-to-all-start.2 = ((bf16[32,2,2048]{2,1,0:T(2,128)(2,1)}), bf16[32,2,2048]{2,1,0:T(2,128)(2,1)S(1)}, u32[]{:S(2)}, u32[]{:S(2)}) async-start(bf16[32,2,2048]{2,1,0:T(2,128)(2,1)} %reshape.345), calls=%async_computation.2 | async-start | bytes 524288 | tf_op jit(solution)/shard_map/all_to_all | solution.py:204
  95.0 1.1 all_to_all.38
  96.1 10.5 %all-to-all-done.2 = bf16[32,2,2048]{2,1,0:T(2,128)(2,1)S(1)} async-done(((bf16[32,2,2048]{2,1,0:T(2,128)(2,1)}), bf16[32,2,2048]{2,1,0:T(2,128)(2,1)S(1)}, u32[]{:S(2)}, u32[]{:S(2)}) %all-to-all-start.2) | async-done | bytes 262176 | tf_op jit(solution)/shard_map/all_to_all | solution.py:204
  106.6 4.5 %all-to-all-start.6 = ((f32[32,1,2064]{2,1,0:T(1,128)}), f32[32,1,2064]{2,1,0:T(1,128)S(1)}, u32[]{:S(2)}, u32[]{:S(2)}) async-start(f32[32,1,2064]{2,1,0:T(1,128)} %all_to_all.38), calls=%async_computation.6 | async-start | bytes 557056 | tf_op jit(solution)/shard_map/all_to_all | solution.py:23
  111.2 0.4 reshape.346
  111.6 0.3 fusion.7
  111.9 0.3 copy.140
  112.2 0.5 convert_element_type.104
  112.7 0.6 copy-done.3
  113.5 0.8 copy-done.4
  114.3 0.4 convolution_convert_fusion
  114.7 0.8 reshape.297
  115.5 6.4 %all-to-all-done.6 = f32[32,1,2064]{2,1,0:T(1,128)S(1)} async-done(((f32[32,1,2064]{2,1,0:T(1,128)}), f32[32,1,2064]{2,1,0:T(1,128)S(1)}, u32[]{:S(2)}, u32[]{:S(2)}) %all-to-all-start.6) | async-done | bytes 264224 | tf_op jit(solution)/shard_map/all_to_all | solution.py:23
  121.9 7.8 %all-to-all-start.3 = ((bf16[16,4,2048]{2,1,0:T(4,128)(2,1)}), bf16[16,4,2048]{2,1,0:T(4,128)(2,1)S(1)}, u32[]{:S(2)}, u32[]{:S(2)}) async-start(bf16[16,4,2048]{2,1,0:T(4,128)(2,1)} %reshape.297), calls=%async_computation.3 | async-start | bytes 524288 | tf_op jit(solution)/shard_map/all_to_all | solution.py:64
  129.9 11.4 %all-to-all-done.3 = bf16[16,4,2048]{2,1,0:T(4,128)(2,1)S(1)} async-done(((bf16[16,4,2048]{2,1,0:T(4,128)(2,1)}), bf16[16,4,2048]{2,1,0:T(4,128)(2,1)S(1)}, u32[]{:S(2)}, u32[]{:S(2)}) %all-to-all-start.3) | async-done | bytes 262176 | tf_op jit(solution)/shard_map/all_to_all | solution.py:64
  141.3 0.8 broadcast_in_dim.18
  142.1 3.9 %all-to-all-start.7 = ((f32[32,1,2064]{2,1,0:T(1,128)}), f32[32,1,2064]{2,1,0:T(1,128)S(1)}, u32[]{:S(2)}, u32[]{:S(2)}) async-start(f32[32,1,2064]{2,1,0:T(1,128)} %broadcast_in_dim.18), calls=%async_computation.7 | async-start | bytes 557056 | tf_op jit(solution)/shard_map/all_to_all | solution.py:41
  146.1 13.0 %all-to-all-done.7 = f32[32,1,2064]{2,1,0:T(1,128)S(1)} async-done(((f32[32,1,2064]{2,1,0:T(1,128)}), f32[32,1,2064]{2,1,0:T(1,128)S(1)}, u32[]{:S(2)}, u32[]{:S(2)}) %all-to-all-start.7) | async-done | bytes 264224 | tf_op jit(solution)/shard_map/all_to_all | solution.py:41
  159.1 0.8 broadcast_in_dim.16
  159.9 3.9 %all-to-all-start.4 = ((bf16[16,4,2048]{2,1,0:T(4,128)(2,1)}), bf16[16,4,2048]{2,1,0:T(4,128)(2,1)S(1)}, u32[]{:S(2)}, u32[]{:S(2)}) async-start(bf16[16,4,2048]{2,1,0:T(4,128)(2,1)} %broadcast_in_dim.16), calls=%async_computation.4 | async-start | bytes 524288 | tf_op jit(solution)/shard_map/all_to_all | solution.py:41
  164.0 0.7 reduce.7
  165.1 10.5 %all-to-all-done.4 = bf16[16,4,2048]{2,1,0:T(4,128)(2,1)S(1)} async-done(((bf16[16,4,2048]{2,1,0:T(4,128)(2,1)}), bf16[16,4,2048]{2,1,0:T(4,128)(2,1)S(1)}, u32[]{:S(2)}, u32[]{:S(2)}) %all-to-all-start.4) | async-done | bytes 262176 | tf_op jit(solution)/shard_map/all_to_all | solution.py:41
  177.4 1.1 reshape.347
  178.5 4.4 %all-to-all-start.5 = ((bf16[32,2,2048]{2,1,0:T(2,128)(2,1)}), bf16[32,2,2048]{2,1,0:T(2,128)(2,1)S(1)}, u32[]{:S(2)}, u32[]{:S(2)}) async-start(bf16[32,2,2048]{2,1,0:T(2,128)(2,1)} %reshape.347), calls=%async_computation.5 | async-start | bytes 524288 | tf_op jit(solution)/shard_map/all_to_all | solution.py:223
  183.1 15.9 %all-gather.1 = bf16[4096,64]{0,1:T(8,128)(2,1)S(1)} all-gather(bf16[256,64]{0,1:T(8,128)(2,1)S(1)} %convolution_convert_fusion.1), channel_id=3, replica_groups=mesh['ep'=32,'tp'=16] {'tp'}, dimensions={0}, use_global_device_ids=true | all-gather | bytes 557056 | tf_op jit(solution)/shard_map/all_gather | solution.py:58
  199.1 0.3 copy.150
  199.7 0.4 reshape.348
  200.0 3.2 %gather_fusion.1 = bf16[1024,64]{1,0:T(8,128)(2,1)S(1)} fusion(bf16[2048,64]{1,0:T(8,128)(2,1)S(1)} %bitcast.203, s32[1024]{0:T(1024)S(1)} %broadcast_clamp_fusion), kind=kCustom, calls=%fused_computation.1 | custom fusion | bytes 266240 | tf_op jit(solution)/shard_map/gather | solution.py:228
  203.2 0.4 fusion.12
  203.8 0.7 copy.144
  (124 shorter events, 7.2 us)
Async XLA Ops:
  0.6 112.9 %copy-start = (bf16[1,128,2048]{2,1,0:T(8,128)(2,1)S(1)}, bf16[1,128,2048]{2,1,0:T(8,128)(2,1)}, u32[]{:S(2)}) copy-start(bf16[1,128,2048]{2,1,0:T(8,128)(2,1)} %param.33) | copy-start | bytes 1572868
  1.7 0.8 copy-start.5
  1.7 0.8 copy-start.6
  1.7 0.8 copy-start.8
  1.7 0.7 copy-start.9
  1.7 0.7 copy-start.15
  3.7 13.9 %copy-start.17 = (s32[8]{0:T(128)S(1)}, s32[8]{0:T(128)}, u32[]{:S(2)}) copy-start(s32[8]{0:T(128)} %param.29) | copy-start | bytes 100
  3.7 13.9 %copy-start.12 = (s32[256,4]{0,1:T(4,128)S(1)}, s32[256,4]{0,1:T(4,128)}, u32[]{:S(2)}) copy-start(s32[256,4]{0,1:T(4,128)} %param.34) | copy-start | bytes 12292
  3.7 37.4 %all-to-all-start = ((f32[32,8,769]{2,1,0:T(8,128)}), f32[32,8,769]{2,1,0:T(8,128)S(1)}, u32[]{:S(2)}, u32[]{:S(2)}) async-start(f32[32,8,769]{2,1,0:T(8,128)} %pad_maximum_fusion), calls=%async_computation | async-start | bytes 1835008 | tf_op jit(solution)/shard_map/all_to_all | solution.py:23
  17.6 24.1 %copy-start.2 = (f32[8,1,128,256]{3,2,1,0:T(8,128)S(1)}, f32[8,1,128,256]{3,2,1,0:T(8,128)}, u32[]{:S(2)}) copy-start(f32[8,1,128,256]{3,2,1,0:T(8,128)} %param.28) | copy-start | bytes 3145732
  41.9 39.3 %copy-start.1 = (f32[8,1,128,256]{3,2,1,0:T(8,128)}, f32[8,1,128,256]{3,2,1,0:T(8,128)S(1)}, u32[]{:S(2)}) copy-start(f32[8,1,128,256]{3,2,1,0:T(8,128)S(1)} %multiply_add_fusion) | copy-start | bytes 3145732
  43.4 15.4 %all-to-all-start.1 = ((bf16[32,8,256]{2,1,0:T(8,128)(2,1)}), bf16[32,8,256]{2,1,0:T(8,128)(2,1)S(1)}, u32[]{:S(2)}, u32[]{:S(2)}) async-start(bf16[32,8,256]{2,1,0:T(8,128)(2,1)} %broadcast_in_dim.13), calls=%async_computation.1 | async-start | bytes 262144 | tf_op jit(solution)/shard_map/all_to_all | solution.py:41
  49.4 0.7 copy-start.13
  49.4 9.4 %copy-start.7 = (bf16[256,64]{0,1:T(8,128)(2,1)S(1)}, bf16[256,64]{0,1:T(8,128)(2,1)}, u32[]{:S(2)}) copy-start(bf16[256,64]{0,1:T(8,128)(2,1)} %param.27) | copy-start | bytes 98308
  81.9 0.7 copy-start.10
  81.9 0.7 copy-start.11
  82.8 0.7 copy-start.18
  90.9 15.7 %all-to-all-start.2 = ((bf16[32,2,2048]{2,1,0:T(2,128)(2,1)}), bf16[32,2,2048]{2,1,0:T(2,128)(2,1)S(1)}, u32[]{:S(2)}, u32[]{:S(2)}) async-start(bf16[32,2,2048]{2,1,0:T(2,128)(2,1)} %reshape.345), calls=%async_computation.2 | async-start | bytes 524288 | tf_op jit(solution)/shard_map/all_to_all | solution.py:204
  106.6 15.3 %all-to-all-start.6 = ((f32[32,1,2064]{2,1,0:T(1,128)}), f32[32,1,2064]{2,1,0:T(1,128)S(1)}, u32[]{:S(2)}, u32[]{:S(2)}) async-start(f32[32,1,2064]{2,1,0:T(1,128)} %all_to_all.38), calls=%async_computation.6 | async-start | bytes 557056 | tf_op jit(solution)/shard_map/all_to_all | solution.py:23
  112.2 1.0 copy-start.3
  113.3 1.0 copy-start.4
  121.9 19.4 %all-to-all-start.3 = ((bf16[16,4,2048]{2,1,0:T(4,128)(2,1)}), bf16[16,4,2048]{2,1,0:T(4,128)(2,1)S(1)}, u32[]{:S(2)}, u32[]{:S(2)}) async-start(bf16[16,4,2048]{2,1,0:T(4,128)(2,1)} %reshape.297), calls=%async_computation.3 | async-start | bytes 524288 | tf_op jit(solution)/shard_map/all_to_all | solution.py:64
  142.1 17.0 %all-to-all-start.7 = ((f32[32,1,2064]{2,1,0:T(1,128)}), f32[32,1,2064]{2,1,0:T(1,128)S(1)}, u32[]{:S(2)}, u32[]{:S(2)}) async-start(f32[32,1,2064]{2,1,0:T(1,128)} %broadcast_in_dim.18), calls=%async_computation.7 | async-start | bytes 557056 | tf_op jit(solution)/shard_map/all_to_all | solution.py:41
  159.9 3.9 %copy-start.14 = (f32[256,4]{0,1:T(4,128)S(1)}, f32[256,4]{0,1:T(4,128)}, u32[]{:S(2)}) copy-start(f32[256,4]{0,1:T(4,128)} %param.35) | copy-start | bytes 12292
  159.9 15.7 %all-to-all-start.4 = ((bf16[16,4,2048]{2,1,0:T(4,128)(2,1)}), bf16[16,4,2048]{2,1,0:T(4,128)(2,1)S(1)}, u32[]{:S(2)}, u32[]{:S(2)}) async-start(bf16[16,4,2048]{2,1,0:T(4,128)(2,1)} %broadcast_in_dim.16), calls=%async_computation.4 | async-start | bytes 524288 | tf_op jit(solution)/shard_map/all_to_all | solution.py:41
  178.5 4.4 %copy-start.16 = (bf16[128,64]{0,1:T(8,128)(2,1)S(1)}, bf16[128,64]{0,1:T(8,128)(2,1)}, u32[]{:S(2)}) copy-start(bf16[128,64]{0,1:T(8,128)(2,1)} %param.38) | copy-start | bytes 49156
  178.5 21.2 %all-to-all-start.5 = ((bf16[32,2,2048]{2,1,0:T(2,128)(2,1)}), bf16[32,2,2048]{2,1,0:T(2,128)(2,1)S(1)}, u32[]{:S(2)}, u32[]{:S(2)}) async-start(bf16[32,2,2048]{2,1,0:T(2,128)(2,1)} %reshape.347), calls=%async_computation.5 | async-start | bytes 524288 | tf_op jit(solution)/shard_map/all_to_all | solution.py:223
